TPU v7x, 32 devices: a whole 2x2x4 slice. The times are simulated.
32 devices in a mesh: ep: 8 (over z, core), tp: 4 (over y, x).
Axes of the slice: x: 2, y: 2, z: 4, core: 2. Of those that a mesh axis runs over, the one named last changes fastest.
Arguments:
- query_rows: bfloat16 [3072, 2048], P('ep', 'tp'), may hold values from -6 to 6
- key_rows: bfloat16 [3072, 2048], P('ep', 'tp'), may hold values from -6 to 6
- value_rows: bfloat16 [3072, 2048], P('ep', 'tp'), may hold values from -6 to 6
- second_scale: float32 [16], P('tp'), may hold values from 0.3 to 0.8
- head_gain: float32 [128], replicated, may hold values from 0.1 to 1.9
- out_weight: bfloat16 [2048, 4096], P(None, 'tp'), may hold values from -0.125 to 0.125
- routed_rows: bfloat16 [1024, 4096], P('ep', 'tp'), may hold values from -6 to 6
- norm_gain: float32 [4096], replicated, may hold values from 0.1 to 1.9
- route_ids: int32 [1024, 2], P('ep'), may hold values from 0 to 7, all different within a row; in each aligned block of 128 rows (0 to 127, 128 to 255, ...) at most 64 rows name the same one
- route_weight: float32 [1024, 2], P('ep'), may hold values from 0.1 to 0.9
- expert_gate: bfloat16 [8, 4096, 2048], P('ep', None, 'tp'), may hold values from -0.09375 to 0.09375
- expert_up: bfloat16 [8, 4096, 2048], P('ep', None, 'tp'), may hold values from -0.09375 to 0.09375
- expert_down: bfloat16 [8, 2048, 4096], P('ep', None, 'tp'), may hold values from -0.125 to 0.125
Outputs:
- mixer_out: bfloat16 [3072, 4096], P('ep', 'tp')
- expert_mix: bfloat16 [1024, 4096], P('ep', 'tp')
Inputs may be any that keep to these rules, and one draw needn't show every extreme that they name: `route_ids`: among the 128 tokens of one index of ep, no expert is named by more than 64 of them, a bound that some block reaches.
All inputs are finite; a program needn't handle non-finite values.
Results may differ from a plain program's by a relative error of at most 0.0085.
Values may be sent and summed in bfloat16 or wider, within the bound.
No kernel may reach another device: no remote copies, remote signals or barrier semaphores. Data moves between devices by JAX's collectives and lax.ppermute only.
A program may use at most 128 MiB of HBM per device.

v0:
```python
import jax
import jax.numpy as jnp
from jax import lax
from jax.sharding import PartitionSpec as P

eps = 1e-06
head_factor = 0.8
neg_big = -1e30
key_block_rows = 1024


def rms_rows(rows_in, gain):
    floats = rows_in.astype(jnp.float32)
    factor = lax.rsqrt(jnp.mean(floats * floats, axis=-1, keepdims=True) + eps)
    return (floats * factor * gain).astype(jnp.bfloat16)


def per_device(
    query_rows,
    key_rows,
    value_rows,
    second_scale,
    head_gain,
    out_weight,
    routed_rows,
    norm_gain,
    route_ids,
    route_weight,
    expert_gate,
    expert_up,
    expert_down,
):
    count_a = query_rows.shape[0]
    per_head = second_scale.shape[0]
    head_dim = query_rows.shape[1] // (2 * per_head)
    value_dim = head_gain.shape[0]
    query_four = query_rows.reshape(count_a, per_head, 2, head_dim)
    query_pos = lax.axis_index("ep") * count_a + jnp.arange(count_a, dtype=jnp.int32)

    def key_block(carry_state, key_part, value_part, block_start):
        key_count = key_part.shape[0]
        key_four = key_part.reshape(key_count, per_head, 2, head_dim)
        value_three = value_part.reshape(key_count, per_head, value_dim)
        scores = jnp.einsum(
            "ihcd,jhcd->ihcj", query_four, key_four, preferred_element_type=jnp.float32
        ) * head_dim ** (-0.5)
        allowed = (
            query_pos[:, None] >= block_start + jnp.arange(key_count, dtype=jnp.int32)[None, :]
        )[:, None, None, :]
        scores = jnp.where(allowed, scores, neg_big)
        old_max, old_sum, old_acc = carry_state
        new_max = jnp.maximum(old_max, jnp.max(scores, axis=-1))
        weights = jnp.where(allowed, jnp.exp(scores - new_max[..., None]), 0.0)
        shrink = jnp.exp(old_max - new_max)
        new_sum = old_sum * shrink + jnp.sum(weights, axis=-1)
        update = jnp.einsum(
            "ihcj,jhe->ihce",
            weights.astype(jnp.bfloat16),
            value_three,
            preferred_element_type=jnp.float32,
        )
        return (new_max, new_sum, old_acc * shrink[..., None] + update)

    start_state = (
        jnp.full((count_a, per_head, 2), neg_big, jnp.float32),
        jnp.zeros((count_a, per_head, 2), jnp.float32),
        jnp.zeros((count_a, per_head, 2, value_dim), jnp.float32),
    )
    key_part = lax.all_gather(key_rows, "ep", axis=0, tiled=True)
    value_part = lax.all_gather(value_rows, "ep", axis=0, tiled=True)
    key_count = key_part.shape[0]

    def step_block(block_num, inner_state):
        offset_rows = block_num * key_block_rows
        key_slice = lax.dynamic_slice_in_dim(key_part, offset_rows, key_block_rows, 0)
        value_slice = lax.dynamic_slice_in_dim(value_part, offset_rows, key_block_rows, 0)
        return key_block(inner_state, key_slice, value_slice, offset_rows)

    run_max, run_sum, run_acc = lax.fori_loop(
        0, key_count // key_block_rows, step_block, start_state
    )
    maps_both = run_acc / run_sum[..., None]
    mixed_maps = maps_both[:, :, 0] - second_scale[None, :, None] * maps_both[:, :, 1]
    mean_sq = jnp.mean(mixed_maps * mixed_maps, axis=-1, keepdims=True)
    head_out = (
        (mixed_maps * lax.rsqrt(mean_sq + eps) * head_gain * head_factor)
        .astype(jnp.bfloat16)
        .reshape(count_a, per_head * value_dim)
    )
    count_b = routed_rows.shape[0]
    route_count = route_ids.shape[1]
    experts_here = expert_gate.shape[0]
    ep_devices = lax.axis_size("ep")
    expert_total = experts_here * ep_devices
    capacity = 2 * count_b * route_count // expert_total
    flat_expert = route_ids.reshape(-1)
    chosen = (flat_expert[:, None] == jnp.arange(expert_total, dtype=jnp.int32)[None, :]).astype(
        jnp.int32
    )
    ranks = jnp.sum((jnp.cumsum(chosen, axis=0) - 1) * chosen, axis=1)
    slot_of = flat_expert * capacity + ranks
    token_of = jnp.arange(count_b * route_count, dtype=jnp.int32) // route_count
    slot_token = jnp.full((expert_total * capacity,), count_b, jnp.int32).at[slot_of].set(token_of)
    padded = jnp.concatenate(
        [routed_rows, jnp.zeros((1, routed_rows.shape[1]), jnp.bfloat16)], axis=0
    )
    outgoing = padded[slot_token].reshape(ep_devices, experts_here, capacity, routed_rows.shape[1])
    column_parts = lax.all_to_all(outgoing, "ep", split_axis=0, concat_axis=0, tiled=True)
    arrived = rms_rows(lax.all_gather(column_parts, "tp", axis=3, tiled=True), norm_gain)
    gate_val = jnp.einsum(
        "sxcd,xdf->sxcf", arrived, expert_gate, preferred_element_type=jnp.float32
    )
    up_val = jnp.einsum("sxcd,xdf->sxcf", arrived, expert_up, preferred_element_type=jnp.float32)
    hidden = (jax.nn.silu(gate_val) * up_val).astype(jnp.bfloat16)
    weight_rows = out_weight
    attn_total = jnp.dot(
        lax.all_gather(
            head_out.reshape(1, 1, count_a, head_out.shape[1]), "tp", axis=3, tiled=True
        )[0, 0],
        weight_rows,
        preferred_element_type=jnp.float32,
    )
    weight_rows = expert_down
    moe_total = jnp.einsum(
        "sxcf,xfd->sxcd",
        lax.all_gather(hidden, "tp", axis=3, tiled=True),
        weight_rows,
        preferred_element_type=jnp.float32,
    )
    mixer_out = attn_total.astype(jnp.bfloat16)
    returned = lax.all_to_all(
        moe_total.astype(jnp.bfloat16), "ep", split_axis=0, concat_axis=0, tiled=True
    )
    flat_back = returned.reshape(expert_total * capacity, returned.shape[3])
    picked = flat_back[slot_of].astype(jnp.float32).reshape(count_b, route_count, returned.shape[3])
    expert_mix = jnp.sum(picked * route_weight[:, :, None], axis=1).astype(jnp.bfloat16)
    return (mixer_out, expert_mix)


def solution(mesh):
    placed = (
        P("ep", "tp"),
        P("ep", "tp"),
        P("ep", "tp"),
        P("tp"),
        P(),
        P(None, "tp"),
        P("ep", "tp"),
        P(),
        P("ep", None),
        P("ep", None),
        P("ep", None, "tp"),
        P("ep", None, "tp"),
        P("ep", None, "tp"),
    )
    return jax.shard_map(
        per_device,
        mesh=mesh,
        in_specs=placed,
        out_specs=(P("ep", "tp"), P("ep", "tp")),
        check_vma=False,
    )
```

profile of v0, /device:TPU:0, one launch (start us, length us, event | category | flops | bytes accessed | tf_op | source)
XLA Modules:
  0.0 287.7 jit_solution(6418652989304294273)
XLA Ops:
  7.2 0.7 broadcast_multiply_fusion
  7.9 0.8 copy.36
  9.2 0.6 reduce-window.6
  9.8 0.2 slice_reduce_fusion
  10.2 1.4 scatter_custom_fusion
  11.6 1.0 concatenate.3
  12.6 2.1 gather_fusion
  14.7 33.0 %all_to_all.10 = bf16[8,1,64,1024]{3,2,1,0:T(8,128)(2,1)} all-to-all(bf16[8,1,64,1024]{3,2,1,0:T(8,128)(2,1)S(1)} %bitcast.152), channel_id=1, replica_groups=mesh['ep'=8,'tp'=4] {'ep'}, dimensions={0} | all-to-all | bytes 2097152 | tf_op jit(solution)/shard_map/all_to_all | solution.py:108
  47.7 0.9 copy.31
  48.8 0.9 copy.33
  49.8 1.2 copy.32
  51.1 48.2 %all-gather.12.cloned.1.call-done = bf16[8,1,64,4096]{3,2,1,0:T(8,128)(2,1)} async-done(((bf16[8,1,64,1024]{3,2,1,0:T(8,128)(2,1)}), bf16[8,1,64,4096]{3,2,1,0:T(8,128)(2,1)}) %all-gather.12.cloned.1.call-update) | async-done | bytes 4194320 | tf_op jit(solution)/shard_map/all_gather | solution.py:109
  99.4 3.2 %fusion.15 = f32[8,64]{1,0:T(8,128)S(1)} fusion(bf16[8,1,64,4096]{3,2,1,0:T(8,128)(2,1)} %all-gather.12.cloned.1.call-done), kind=kLoop, calls=%fused_computation.28 | loop fusion | flops 6290944 | bytes 4196352 | tf_op jit(solution)/shard_map/reduce_sum | solution.py:14
  102.6 0.2 copy-done.1
  102.8 4.7 %fusion.43 = f32[8,1,64,512]{3,2,0,1:T(8,128)S(1)} fusion(bf16[1,4096,512]{2,1,0:T(8,128)(2,1)} %param.25, bf16[8,1,64,4096]{3,2,1,0:T(8,128)(2,1)S(1)} %copy-done.1, f32[4096]{0:T(1024)S(1)} %copy-done.8, f32[8,64]{1,0:T(8,128)S(1)} %add_rsqrt_fusion.1), kind=kOutput, calls=%fused_computation.44 | convolution fusion | flops 2155872256 | bytes 9455616 | tf_op jit(solution)/shard_map/sxcd,xdf->sxcf/dot_general | solution.py:110
  107.5 3.3 %fusion.58 = bf16[8,1,64,512]{3,2,0,1:T(8,128)(2,1)} fusion(bf16[1,4096,512]{2,1,0:T(8,128)(2,1)S(1)} %copy-done.7, bf16[8,1,64,4096]{3,2,1,0:T(8,128)(2,1)S(1)} %copy-done.1, f32[4096]{0:T(1024)S(1)} %copy-done.8, f32[8,64]{1,0:T(8,128)S(1)} %add_rsqrt_fusion.1, f32[8,1,64,512]{3,2,0,1:T(8,128)S(1)} %fusion.43), kind=kOutput, calls=%fused_computation.47 | convolution fusion | flops 2157445120 | bytes 9979904 | tf_op jit(solution)/shard_map/sxcd,xdf->sxcf/dot_general | solution.py:113
  110.8 0.2 all-gather.10.cloned.1.call-start
  111.0 27.7 %all-gather.6.cloned.1.call-done = bf16[3072,512]{0,1:T(8,128)(2,1)} async-done(((bf16[384,512]{0,1:T(8,128)(2,1)}), bf16[3072,512]{0,1:T(8,128)(2,1)}) %all-gather.6.cloned.1.call-update) | async-done | bytes 3145744 | tf_op jit(solution)/shard_map/all_gather | solution.py:69
  138.8 38.8 %all-gather.8.cloned.1.call-done = bf16[3072,512]{0,1:T(8,128)(2,1)} async-done(((bf16[384,512]{0,1:T(8,128)(2,1)}), bf16[3072,512]{0,1:T(8,128)(2,1)}) %all-gather.8.cloned.1.call-update) | async-done | bytes 3145744 | tf_op jit(solution)/shard_map/all_gather | solution.py:70
  177.5 61.9 %while.18 = (s32[]{:T(128)}, f32[384,4,2]{0,2,1:T(2,128)S(1)}, f32[384,4,2]{0,2,1:T(2,128)S(1)}, f32[384,4,2,128]{0,3,2,1:T(8,128)S(1)}, bf16[3072,512]{0,1:T(8,...) while((s32[]{:T(128)}, f32[384,4,2]{0,2,1:T(2,128)S(1)}, ...), condition=%wide.region_3.4_spmd.clone, body=%wide.region_0.3_spmd.clone.sunk | while | flops 1250443648 | bytes 99691744 | solution.py:79
  177.5 0.3 broadcast_compare_fusion.2
  177.8 1.7 constant_dynamic-slice_fusion.3
  179.5 6.7 %fusion.86 = (f32[384,4,2]{0,2,1:T(2,128)S(1)}, f32[4,2,1024,384]{3,2,1,0:T(8,128)}) fusion(pred[384,1024]{0,1:T(8,128)(4,1)S(1)} %broadcast_compare_fusion.2, bf16[1024,4,2,64]{0,3,2,1:T(8,128)(2,1)S(1)} %bitcast.148, bf16[384,4,2,64]{0,3,2,1:T(8,128)(2,1)S(1)} %get-tuple-element.290), kind=kOutput, calls=%fused_computation.6.clone.1 | convolution fusion | flops 412087296 | bytes 14430208 | tf_op jit(solution)/shard_map/while/body/eval_jaxpr/ihcd,jhcd->ihcj/dot_general | solution.py:44
  186.2 7.0 %fusion.88 = f32[384,4,2]{0,2,1:T(2,128)S(1)} fusion(f32[4,2,1024,384]{3,2,1,0:T(8,128)} %get-tuple-element.257, f32[384,4,2]{0,2,1:T(2,128)S(1)} %fusion.87, pred[384,1024]{0,1:T(8,128)(4,1)S(1)} %broadcast_compare_fusion.2), kind=kLoop, calls=%fused_computation.8.clone.1 | loop fusion | flops 15725568 | bytes 13000704 | tf_op jit(solution)/shard_map/while/body/eval_jaxpr/reduce_sum | solution.py:55
  193.2 1.5 copy-done
  194.7 3.6 %bitcast_add_fusion.2 = f32[384,4,2,128]{0,3,2,1:T(8,128)S(1)} fusion(f32[384,4,2,128]{0,3,2,1:T(8,128)S(1)} %get-tuple-element.276, bf16[1024,4,128,1]{0,2,3,1:T(8,128)(2,1)S(1)} %bitcast.149, f32[4,2,1024,384]{3,2,1,0:T(8,128)S(1)} %copy-done, f32[384,4,2]{0,2,1:T(2,128)S(1)} %fusion.87, pred[384,1024]{0,1:T(8,128)(4,1)S(1)} %broadcast_compare_fusion.2, ...), kind=kOutput, calls=%fused_computation.11.clone.1 | convolution fusion | flops 822214656 | bytes 17195008 | tf_op jit(solution)/shard_map/while/body/eval_jaxpr/ihcj,jhe->ihce/dot_general | solution.py:56
  198.3 0.3 broadcast_compare_fusion.2
  198.6 1.7 constant_dynamic-slice_fusion.3
  200.3 6.7 %fusion.86 = (f32[384,4,2]{0,2,1:T(2,128)S(1)}, f32[4,2,1024,384]{3,2,1,0:T(8,128)}) fusion(pred[384,1024]{0,1:T(8,128)(4,1)S(1)} %broadcast_compare_fusion.2, bf16[1024,4,2,64]{0,3,2,1:T(8,128)(2,1)S(1)} %bitcast.148, bf16[384,4,2,64]{0,3,2,1:T(8,128)(2,1)S(1)} %get-tuple-element.290), kind=kOutput, calls=%fused_computation.6.clone.1 | convolution fusion | flops 412087296 | bytes 14430208 | tf_op jit(solution)/shard_map/while/body/eval_jaxpr/ihcd,jhcd->ihcj/dot_general | solution.py:44
  207.0 6.8 %fusion.88 = f32[384,4,2]{0,2,1:T(2,128)S(1)} fusion(f32[4,2,1024,384]{3,2,1,0:T(8,128)} %get-tuple-element.257, f32[384,4,2]{0,2,1:T(2,128)S(1)} %fusion.87, pred[384,1024]{0,1:T(8,128)(4,1)S(1)} %broadcast_compare_fusion.2), kind=kLoop, calls=%fused_computation.8.clone.1 | loop fusion | flops 15725568 | bytes 13000704 | tf_op jit(solution)/shard_map/while/body/eval_jaxpr/reduce_sum | solution.py:55
  213.9 1.4 copy-done
  215.3 3.6 %bitcast_add_fusion.2 = f32[384,4,2,128]{0,3,2,1:T(8,128)S(1)} fusion(f32[384,4,2,128]{0,3,2,1:T(8,128)S(1)} %get-tuple-element.276, bf16[1024,4,128,1]{0,2,3,1:T(8,128)(2,1)S(1)} %bitcast.149, f32[4,2,1024,384]{3,2,1,0:T(8,128)S(1)} %copy-done, f32[384,4,2]{0,2,1:T(2,128)S(1)} %fusion.87, pred[384,1024]{0,1:T(8,128)(4,1)S(1)} %broadcast_compare_fusion.2, ...), kind=kOutput, calls=%fused_computation.11.clone.1 | convolution fusion | flops 822214656 | bytes 17195008 | tf_op jit(solution)/shard_map/while/body/eval_jaxpr/ihcj,jhe->ihce/dot_general | solution.py:56
  218.9 0.3 broadcast_compare_fusion.2
  219.2 1.7 constant_dynamic-slice_fusion.3
  220.9 6.7 %fusion.86 = (f32[384,4,2]{0,2,1:T(2,128)S(1)}, f32[4,2,1024,384]{3,2,1,0:T(8,128)}) fusion(pred[384,1024]{0,1:T(8,128)(4,1)S(1)} %broadcast_compare_fusion.2, bf16[1024,4,2,64]{0,3,2,1:T(8,128)(2,1)S(1)} %bitcast.148, bf16[384,4,2,64]{0,3,2,1:T(8,128)(2,1)S(1)} %get-tuple-element.290), kind=kOutput, calls=%fused_computation.6.clone.1 | convolution fusion | flops 412087296 | bytes 14430208 | tf_op jit(solution)/shard_map/while/body/eval_jaxpr/ihcd,jhcd->ihcj/dot_general | solution.py:44
  227.6 6.8 %fusion.88 = f32[384,4,2]{0,2,1:T(2,128)S(1)} fusion(f32[4,2,1024,384]{3,2,1,0:T(8,128)} %get-tuple-element.257, f32[384,4,2]{0,2,1:T(2,128)S(1)} %fusion.87, pred[384,1024]{0,1:T(8,128)(4,1)S(1)} %broadcast_compare_fusion.2), kind=kLoop, calls=%fused_computation.8.clone.1 | loop fusion | flops 15725568 | bytes 13000704 | tf_op jit(solution)/shard_map/while/body/eval_jaxpr/reduce_sum | solution.py:55
  234.4 1.4 copy-done
  235.9 3.6 %bitcast_add_fusion.2 = f32[384,4,2,128]{0,3,2,1:T(8,128)S(1)} fusion(f32[384,4,2,128]{0,3,2,1:T(8,128)S(1)} %get-tuple-element.276, bf16[1024,4,128,1]{0,2,3,1:T(8,128)(2,1)S(1)} %bitcast.149, f32[4,2,1024,384]{3,2,1,0:T(8,128)S(1)} %copy-done, f32[384,4,2]{0,2,1:T(2,128)S(1)} %fusion.87, pred[384,1024]{0,1:T(8,128)(4,1)S(1)} %broadcast_compare_fusion.2, ...), kind=kOutput, calls=%fused_computation.11.clone.1 | convolution fusion | flops 822214656 | bytes 17195008 | tf_op jit(solution)/shard_map/while/body/eval_jaxpr/ihcj,jhe->ihce/dot_general | solution.py:56
  239.6 0.2 fusion.64
  240.0 1.0 multiply_convert_fusion
  241.0 6.1 %fusion.38 = bf16[8,1,64,1024]{3,2,1,0:T(8,128)(2,1)} fusion(bf16[1,2048,1024]{2,1,0:T(8,128)(2,1)} %param.27, bf16[8,1,64,2048]{3,2,0,1:T(8,128)(2,1)} %all-gather.14.cloned.1.call-done), kind=kOutput, calls=%fused_computation.43 | convolution fusion | flops 2148007936 | bytes 7340032 | tf_op jit(solution)/shard_map/sxcf,xfd->sxcd/dot_general | solution.py:124
  247.2 3.6 %all-to-all-start.1 = ((bf16[8,1,64,1024]{3,2,1,0:T(8,128)(2,1)}), bf16[8,1,64,1024]{3,2,1,0:T(8,128)(2,1)S(1)}, u32[]{:S(2)}, u32[]{:S(2)}) async-start(bf16[8,1,64,1024]{3,2,1,0:T(8,128)(2,1)} %fusion.38), calls=%async_computation.1 | async-start | bytes 2097152 | tf_op jit(solution)/shard_map/all_to_all | solution.py:131
  250.9 20.8 %all-gather.10.cloned.1.call-done = bf16[1,1,384,2048]{2,3,1,0:T(8,128)(2,1)} async-done(((bf16[1,1,384,512]{2,3,1,0:T(8,128)(2,1)}), bf16[1,1,384,2048]{2,3,1,0:T(8,128)(2,1)}) %all-gather.10.cloned.1.call-update) | async-done | bytes 1572880 | tf_op jit(solution)/shard_map/all_gather | solution.py:117
  271.6 5.4 %fusion.35 = bf16[384,1024]{1,0:T(8,128)(2,1)} fusion(bf16[2048,1024]{1,0:T(8,128)(2,1)} %param.20, bf16[1,1,384,2048]{2,3,1,0:T(8,128)(2,1)} %all-gather.10.cloned.1.call-done), kind=kOutput, calls=%fused_computation.42 | convolution fusion | flops 1611005952 | bytes 6553600 | tf_op jit(solution)/shard_map/dot_general | solution.py:116
  277.0 0.2 all-to-all-done.1
  277.2 1.2 gather_fusion.1
  278.4 0.7 reshape.247
  279.0 2.1 multiply_reduce_fusion
  (66 shorter events, 1.7 us)
Async XLA Ops:
  7.2 92.2 %all-gather.12.cloned.1.call-start = ((), (), s32[]{:S(2)}) async-start(), calls=%async_computation.5 | async-start | bytes 5242880 | tf_op jit(solution)/shard_map/all_gather | solution.py:109
  12.6 35.1 %copy-start.2 = (bf16[384,512]{1,0:T(8,128)(2,1)S(1)}, bf16[384,512]{1,0:T(8,128)(2,1)}, u32[]{:S(2)}) copy-start(bf16[384,512]{1,0:T(8,128)(2,1)} %param.16) | copy-start | bytes 1179652
  14.7 34.1 %copy-start.3 = (bf16[384,512]{1,0:T(8,128)(2,1)S(1)}, bf16[384,512]{1,0:T(8,128)(2,1)}, u32[]{:S(2)}) copy-start(bf16[384,512]{1,0:T(8,128)(2,1)} %param.17) | copy-start | bytes 1179652
  14.7 36.3 %copy-start.4 = (f32[4]{0:T(128)S(1)}, f32[4]{0:T(128)}, u32[]{:S(2)}) copy-start(f32[4]{0:T(128)} %param.18) | copy-start | bytes 52
  14.7 36.3 %copy-start.6 = (f32[128]{0:T(128)S(1)}, f32[128]{0:T(128)}, u32[]{:S(2)}) copy-start(f32[128]{0:T(128)} %param.19) | copy-start | bytes 1540
  47.7 54.9 %copy-start.8 = (f32[4096]{0:T(1024)S(1)}, f32[4096]{0:T(1024)}, u32[]{:S(2)}) copy-start(f32[4096]{0:T(1024)} %param.22) | copy-start | bytes 49156
  47.7 91.1 %all-gather.6.cloned.1.call-start = ((), (), s32[]{:S(2)}) async-start(), calls=%async_computation.2 | async-start | bytes 3538944 | tf_op jit(solution)/shard_map/all_gather | solution.py:69
  48.7 128.8 %all-gather.8.cloned.1.call-start = ((), (), s32[]{:S(2)}) async-start(), calls=%async_computation.3 | async-start | bytes 3538944 | tf_op jit(solution)/shard_map/all_gather | solution.py:70
  49.7 191.3 %all-gather.14.cloned.1.call-start = ((), (), s32[]{:S(2)}) async-start(), calls=%async_computation.6 | async-start | bytes 2621440 | tf_op jit(solution)/shard_map/all_gather | solution.py:126
  99.3 3.4 %copy-start.1 = (bf16[8,1,64,4096]{3,2,1,0:T(8,128)(2,1)S(1)}, bf16[8,1,64,4096]{3,2,1,0:T(8,128)(2,1)}, u32[]{:S(2)}) copy-start(bf16[8,1,64,4096]{3,2,1,0:T(8,128)(2,1)} %all-gather.12.cloned.1.call-done) | copy-start | bytes 12582916
  102.8 4.7 %copy-start.7 = (bf16[1,4096,512]{2,1,0:T(8,128)(2,1)S(1)}, bf16[1,4096,512]{2,1,0:T(8,128)(2,1)}, u32[]{:S(2)}) copy-start(bf16[1,4096,512]{2,1,0:T(8,128)(2,1)} %param.26) | copy-start | bytes 12582916
  110.8 160.8 %all-gather.10.cloned.1.call-start = ((), (), s32[]{:S(2)}) async-start(), calls=%async_computation.4 | async-start | bytes 1966080 | tf_op jit(solution)/shard_map/all_gather | solution.py:117
  186.2 8.5 %copy-start = (f32[4,2,1024,384]{3,2,1,0:T(8,128)S(1)}, f32[4,2,1024,384]{3,2,1,0:T(8,128)}, u32[]{:S(2)}) copy-start(f32[4,2,1024,384]{3,2,1,0:T(8,128)} %get-tuple-element.257) | copy-start | bytes 37748740 | tf_op jit(solution)/shard_map/while
  207.0 8.3 %copy-start = (f32[4,2,1024,384]{3,2,1,0:T(8,128)S(1)}, f32[4,2,1024,384]{3,2,1,0:T(8,128)}, u32[]{:S(2)}) copy-start(f32[4,2,1024,384]{3,2,1,0:T(8,128)} %get-tuple-element.257) | copy-start | bytes 37748740 | tf_op jit(solution)/shard_map/while
  227.6 8.3 %copy-start = (f32[4,2,1024,384]{3,2,1,0:T(8,128)S(1)}, f32[4,2,1024,384]{3,2,1,0:T(8,128)}, u32[]{:S(2)}) copy-start(f32[4,2,1024,384]{3,2,1,0:T(8,128)} %get-tuple-element.257) | copy-start | bytes 37748740 | tf_op jit(solution)/shard_map/while
  241.0 9.7 %copy-start.5 = (f32[128,2]{0,1:T(2,128)S(1)}, f32[128,2]{0,1:T(2,128)}, u32[]{:S(2)}) copy-start(f32[128,2]{0,1:T(2,128)} %param.24) | copy-start | bytes 3076
  247.2 30.1 %all-to-all-start.1 = ((bf16[8,1,64,1024]{3,2,1,0:T(8,128)(2,1)}), bf16[8,1,64,1024]{3,2,1,0:T(8,128)(2,1)S(1)}, u32[]{:S(2)}, u32[]{:S(2)}) async-start(bf16[8,1,64,1024]{3,2,1,0:T(8,128)(2,1)} %fusion.38), calls=%async_computation.1 | async-start | bytes 2097152 | tf_op jit(solution)/shard_map/all_to_all | solution.py:131
Sparse Core Ops, SparseCore 0:
  47.8 51.4 all-gather.11
  101.0 37.7 all-gather.5
  140.4 37.0 all-gather.7
  179.8 34.3 all-gather.13
  241.1 30.4 all-gather.9
where the time goes:
time: 288 us
  waiting for transfers between devices  136 us (47%)
  matrix products  50.1 us (17%)
  blocking collectives  33 us (11%)
  other arithmetic  29.5 us (10%)
  local copies, waits for them, and re-layouts  21 us (7%)
  between operations  14 us (5%)
  starting transfers between devices  3.94 us (1%)
    all_gather x1, waiting for transfers between devices, per_device(): lax.all_gather(column_parts, 'tp', axis=3, tiled=True)  48.2 us
    all_gather x1, waiting for transfers between devices, per_device(): value_part = lax.all_gather(value_rows, 'ep', axis=0, tiled=True)  38.8 us
    all_to_all x1, blocking collectives, per_device(): lax.all_to_all(outgoing, 'ep', split_axis=0, concat_axis=0, tiled=True)  33 us
    all_gather x1, waiting for transfers between devices, per_device(): key_part = lax.all_gather(key_rows, 'ep', axis=0, tiled=True)  27.7 us
    all_gather x1, waiting for transfers between devices, per_device(): lax.all_gather(head_out.reshape(1, 1, count_a, head_out.shape[1]), 'tp',...  20.8 us
    reduce_sum x3, other arithmetic, key_block(): new_sum = old_sum * shrink + jnp.sum(weights, axis=-1)  20.5 us
    dot_general x3, matrix products, key_block(): jnp.einsum('ihcd,jhcd->ihcj', query_four, key_four, preferred_element_typ...  20 us
    dot_general x3, matrix products, key_block(): jnp.einsum('ihcj,jhe->ihce', weights.astype(jnp.bfloat16), value_three, p...  10.7 us
  transfers between devices with their start and end apart: 6, of which 5 were waited for; matrix products, arithmetic and copies ran while one was open for 29% of the time, Pallas kernels for 0%

commit v1 on v0

--- a/solution.py
+++ b/solution.py
@@ -67,7 +67,12 @@
         jnp.zeros((count_a, per_head, 2, value_dim), jnp.float32),
     )
     key_part = lax.all_gather(key_rows, "ep", axis=0, tiled=True)
-    value_part = lax.all_gather(value_rows, "ep", axis=0, tiled=True)
+    ring = [value_rows]
+    for hop in range(7):
+        ring.append(lax.ppermute(ring[-1], "ep", [(dev, (dev + 1) % 8) for dev in range(8)]))
+    value_part = jnp.roll(
+        jnp.concatenate(ring[::-1], axis=0), (lax.axis_index("ep") + 1) * ring[0].shape[0], axis=0
+    )
     key_count = key_part.shape[0]
 
     def step_block(block_num, inner_state):

time: 288 us -> 250 us (0.87)
  waiting for transfers between devices: 136 us -> 83.4 us
  local copies, waits for them, and re-layouts: 21 us -> 33.3 us
    ppermute x0 -> x7, waiting for transfers between devices: none -> 61.1 us  [per_device(): lax.ppermute(ring[-1], 'ep', [(dev, (dev + 1) % 8) for dev in range(8)])]
    all_gather x1, waiting for transfers between devices: 48.2 us -> 0.01 us  [per_device(): lax.all_gather(column_parts, 'tp', axis=3, tiled=True)]
    all_gather x1 -> x0, waiting for transfers between devices: 38.8 us -> none  [per_device(): value_part = lax.all_gather(value_rows, 'ep', axis=0, tiled=True)]
    all_gather x1, waiting for transfers between devices: 27.7 us -> 1.25 us  [per_device(): key_part = lax.all_gather(key_rows, 'ep', axis=0, tiled=True)]
    unnamed x21 -> x48, local copies, waits for them, and re-layouts: 4.21 us -> 12.4 us
    dynamic_slice x0 -> x1, local copies, waits for them, and re-layouts: none -> 4.08 us  [per_device(): jnp.roll(jnp.concatenate(ring[::-1], axis=0), (lax.axis_index('ep') + 1)...]
  transfers between devices with their start and end apart: 6 -> 12, of which waited for: 5 -> 10; matrix products, arithmetic and copies ran while one was open for 29% -> 39% of each run, Pallas kernels for 0% -> 0%
where the time goes in v1:
time: 250 us; the launch traced here: 249 us
  waiting for transfers between devices  83.4 us (33%)
  matrix products  51.4 us (21%)
  local copies, waits for them, and re-layouts  33.3 us (13%)
  blocking collectives  32.8 us (13%)
  other arithmetic  29.4 us (12%)
  between operations  14.2 us (6%)
  starting transfers between devices  4.01 us (2%)
    ppermute x7, waiting for transfers between devices, per_device(): lax.ppermute(ring[-1], 'ep', [(dev, (dev + 1) % 8) for dev in range(8)])  61.1 us
    all_to_all x1, blocking collectives, per_device(): lax.all_to_all(outgoing, 'ep', split_axis=0, concat_axis=0, tiled=True)  32.8 us
    all_gather x1, waiting for transfers between devices, per_device(): lax.all_gather(head_out.reshape(1, 1, count_a, head_out.shape[1]), 'tp',...  20.6 us
    reduce_sum x3, other arithmetic, key_block(): new_sum = old_sum * shrink + jnp.sum(weights, axis=-1)  20.5 us
    dot_general x3, matrix products, key_block(): jnp.einsum('ihcd,jhcd->ihcj', query_four, key_four, preferred_element_typ...  19.9 us
    unnamed x48, local copies, waits for them, and re-layouts  12.4 us
    dot_general x3, matrix products, key_block(): jnp.einsum('ihcj,jhe->ihce', weights.astype(jnp.bfloat16), value_three, p...  10.7 us
    dot_general x1, matrix products, per_device(): jnp.einsum('sxcf,xfd->sxcd', lax.all_gather(hidden, 'tp', axis=3, tiled=T...  6.14 us
  transfers between devices with their start and end apart: 12, of which 10 were waited for; matrix products, arithmetic and copies ran while one was open for 39% of the time, Pallas kernels for 0%

profile of v1, /device:TPU:0, one launch (start us, length us, event | category | flops | bytes accessed | tf_op | source)
XLA Modules:
  0.0 248.9 jit_solution(13829101176312967507)
XLA Ops:
  10.2 1.4 scatter_custom_fusion
  11.6 1.0 concatenate.10
  12.6 2.1 gather_fusion
  14.7 32.8 %all_to_all.10 = bf16[8,1,64,1024]{3,2,1,0:T(8,128)(2,1)} all-to-all(bf16[8,1,64,1024]{3,2,1,0:T(8,128)(2,1)S(1)} %bitcast.152), channel_id=1, replica_groups=mesh['ep'=8,'tp'=4] {'ep'}, dimensions={0} | all-to-all | bytes 2097152 | tf_op jit(solution)/shard_map/all_to_all | solution.py:113
  47.9 9.0 %collective-permute-done = bf16[384,512]{0,1:T(8,128)(2,1)S(1)} collective-permute-done((bf16[384,512]{0,1:T(8,128)(2,1)S(1)}, bf16[384,512]{0,1:T(8,128)(2,1)S(1)}, u32[]{:S(2)}, u32[]{:S(2)}) %collective-permute-start) | collective-permute-done | bytes 393248 | tf_op jit(solution)/shard_map/ppermute | solution.py:72
  56.9 9.0 %collective-permute-done.1 = bf16[384,512]{0,1:T(8,128)(2,1)S(1)} collective-permute-done((bf16[384,512]{0,1:T(8,128)(2,1)S(1)}, bf16[384,512]{0,1:T(8,128)(2,1)S(1)}, u32[]{:S(2)}, u32[]{:S(2)}) %collective-permute-start.1) | collective-permute-done | bytes 393248 | tf_op jit(solution)/shard_map/ppermute | solution.py:72
  65.9 9.0 %collective-permute-done.2 = bf16[384,512]{0,1:T(8,128)(2,1)S(1)} collective-permute-done((bf16[384,512]{0,1:T(8,128)(2,1)S(1)}, bf16[384,512]{0,1:T(8,128)(2,1)S(1)}, u32[]{:S(2)}, u32[]{:S(2)}) %collective-permute-start.2) | collective-permute-done | bytes 393248 | tf_op jit(solution)/shard_map/ppermute | solution.py:72
  75.6 9.0 %collective-permute-done.3 = bf16[384,512]{0,1:T(8,128)(2,1)S(1)} collective-permute-done((bf16[384,512]{0,1:T(8,128)(2,1)S(1)}, bf16[384,512]{0,1:T(8,128)(2,1)S(1)}, u32[]{:S(2)}, u32[]{:S(2)}) %collective-permute-start.3) | collective-permute-done | bytes 393248 | tf_op jit(solution)/shard_map/ppermute | solution.py:72
  84.6 0.9 copy.35
  85.6 8.0 %collective-permute-done.4 = bf16[384,512]{0,1:T(8,128)(2,1)S(1)} collective-permute-done((bf16[384,512]{0,1:T(8,128)(2,1)S(1)}, bf16[384,512]{0,1:T(8,128)(2,1)S(1)}, u32[]{:S(2)}, u32[]{:S(2)}) %collective-permute-start.4) | collective-permute-done | bytes 393248 | tf_op jit(solution)/shard_map/ppermute | solution.py:72
  93.6 9.1 %collective-permute-done.5 = bf16[384,512]{0,1:T(8,128)(2,1)} collective-permute-done((bf16[384,512]{0,1:T(8,128)(2,1)S(1)}, bf16[384,512]{0,1:T(8,128)(2,1)}, u32[]{:S(2)}, u32[]{:S(2)}) %collective-permute-start.5) | collective-permute-done | bytes 393248 | tf_op jit(solution)/shard_map/ppermute | solution.py:72
  102.8 1.2 copy.36
  104.1 8.0 %collective-permute-done.6 = bf16[384,512]{0,1:T(8,128)(2,1)} collective-permute-done((bf16[384,512]{0,1:T(8,128)(2,1)}, bf16[384,512]{0,1:T(8,128)(2,1)}, u32[]{:S(2)}, u32[]{:S(2)}) %collective-permute-start.6) | collective-permute-done | bytes 393248 | tf_op jit(solution)/shard_map/ppermute | solution.py:72
  112.1 1.1 constant_dynamic-update-slice_fusion.15
  113.2 1.1 constant_dynamic-update-slice_fusion.14
  114.3 1.1 constant_dynamic-update-slice_fusion.13
  115.4 1.1 constant_dynamic-update-slice_fusion.12
  116.5 1.1 constant_dynamic-update-slice_fusion.11
  117.9 1.1 constant_dynamic-update-slice_fusion.7
  119.0 1.1 constant_dynamic-update-slice_fusion.6
  120.7 4.1 %constant_dynamic-slice_fusion.2 = bf16[3072,512]{0,1:T(8,128)(2,1)} fusion(bf16[6144,512]{0,1:T(8,128)(2,1)S(1)} %constant_dynamic-update-slice_fusion, s32[]{:T(128)S(6)} %select_n.56), kind=kLoop, calls=%fused_computation.92 | loop fusion | bytes 6291460 | tf_op jit(solution)/shard_map/jit(_roll_dynamic)/dynamic_slice | solution.py:73
  124.7 3.1 %fusion.15 = f32[8,64]{1,0:T(8,128)S(1)} fusion(bf16[8,1,64,4096]{3,2,1,0:T(8,128)(2,1)} %all-gather.9.cloned.1.call-done), kind=kLoop, calls=%fused_computation.28 | loop fusion | flops 6290944 | bytes 4196352 | tf_op jit(solution)/shard_map/reduce_sum | solution.py:14
  127.9 6.0 %fusion.43 = f32[8,1,64,512]{3,2,0,1:T(8,128)S(1)} fusion(bf16[1,4096,512]{2,1,0:T(8,128)(2,1)} %param.25, bf16[8,1,64,4096]{3,2,1,0:T(8,128)(2,1)} %all-gather.9.cloned.1.call-done, f32[4096]{0:T(1024)S(1)} %copy-done.14, f32[8,64]{1,0:T(8,128)S(1)} %add_rsqrt_fusion.1), kind=kOutput, calls=%fused_computation.44 | convolution fusion | flops 2155872256 | bytes 9455616 | tf_op jit(solution)/shard_map/sxcd,xdf->sxcf/dot_general | solution.py:115
  134.0 3.3 %fusion.58 = bf16[8,1,64,512]{3,2,0,1:T(8,128)(2,1)} fusion(bf16[1,4096,512]{2,1,0:T(8,128)(2,1)S(1)} %copy-done.13, bf16[8,1,64,4096]{3,2,1,0:T(8,128)(2,1)S(1)} %copy-done.1, f32[4096]{0:T(1024)S(1)} %copy-done.14, f32[8,64]{1,0:T(8,128)S(1)} %add_rsqrt_fusion.1, f32[8,1,64,512]{3,2,0,1:T(8,128)S(1)} %fusion.43), kind=kOutput, calls=%fused_computation.47 | convolution fusion | flops 2157445120 | bytes 9979904 | tf_op jit(solution)/shard_map/sxcd,xdf->sxcf/dot_general | solution.py:118
  137.5 1.3 all-gather.5.cloned.1.call-done
  138.8 61.9 %while.18 = (s32[]{:T(128)}, f32[384,4,2]{0,2,1:T(2,128)S(1)}, f32[384,4,2]{0,2,1:T(2,128)S(1)}, f32[384,4,2,128]{0,3,2,1:T(8,128)S(1)}, bf16[3072,512]{0,1:T(8,...) while((s32[]{:T(128)}, f32[384,4,2]{0,2,1:T(2,128)S(1)}, ...), condition=%wide.region_3.4_spmd.clone, body=%wide.region_0.3_spmd.clone.sunk | while | flops 1250443648 | bytes 99691728 | solution.py:84
  138.8 1.7 constant_dynamic-slice_fusion.4
  140.8 6.6 %fusion.86 = (f32[384,4,2]{0,2,1:T(2,128)S(1)}, f32[4,2,1024,384]{3,2,1,0:T(8,128)}) fusion(pred[384,1024]{0,1:T(8,128)(4,1)S(1)} %broadcast_compare_fusion.2, bf16[1024,4,2,64]{0,3,2,1:T(8,128)(2,1)S(1)} %bitcast.148, bf16[384,4,2,64]{0,3,2,1:T(8,128)(2,1)S(1)} %get-tuple-element.290), kind=kOutput, calls=%fused_computation.6.clone.1 | convolution fusion | flops 412087296 | bytes 14430208 | tf_op jit(solution)/shard_map/while/body/eval_jaxpr/ihcd,jhcd->ihcj/dot_general | solution.py:44
  147.5 6.9 %fusion.88 = f32[384,4,2]{0,2,1:T(2,128)S(1)} fusion(f32[4,2,1024,384]{3,2,1,0:T(8,128)} %get-tuple-element.257, f32[384,4,2]{0,2,1:T(2,128)S(1)} %fusion.87, pred[384,1024]{0,1:T(8,128)(4,1)S(1)} %broadcast_compare_fusion.2), kind=kLoop, calls=%fused_computation.8.clone.1 | loop fusion | flops 15725568 | bytes 13000704 | tf_op jit(solution)/shard_map/while/body/eval_jaxpr/reduce_sum | solution.py:55
  154.5 1.5 copy-done
  155.9 3.6 %bitcast_add_fusion.2 = f32[384,4,2,128]{0,3,2,1:T(8,128)S(1)} fusion(f32[384,4,2,128]{0,3,2,1:T(8,128)S(1)} %get-tuple-element.276, bf16[1024,4,128,1]{0,2,3,1:T(8,128)(2,1)S(1)} %bitcast.149, f32[4,2,1024,384]{3,2,1,0:T(8,128)S(1)} %copy-done, f32[384,4,2]{0,2,1:T(2,128)S(1)} %fusion.87, pred[384,1024]{0,1:T(8,128)(4,1)S(1)} %broadcast_compare_fusion.2, ...), kind=kOutput, calls=%fused_computation.11.clone.1 | convolution fusion | flops 822214656 | bytes 17195008 | tf_op jit(solution)/shard_map/while/body/eval_jaxpr/ihcj,jhe->ihce/dot_general | solution.py:56
  159.6 1.7 constant_dynamic-slice_fusion.4
  161.6 6.6 %fusion.86 = (f32[384,4,2]{0,2,1:T(2,128)S(1)}, f32[4,2,1024,384]{3,2,1,0:T(8,128)}) fusion(pred[384,1024]{0,1:T(8,128)(4,1)S(1)} %broadcast_compare_fusion.2, bf16[1024,4,2,64]{0,3,2,1:T(8,128)(2,1)S(1)} %bitcast.148, bf16[384,4,2,64]{0,3,2,1:T(8,128)(2,1)S(1)} %get-tuple-element.290), kind=kOutput, calls=%fused_computation.6.clone.1 | convolution fusion | flops 412087296 | bytes 14430208 | tf_op jit(solution)/shard_map/while/body/eval_jaxpr/ihcd,jhcd->ihcj/dot_general | solution.py:44
  168.2 6.8 %fusion.88 = f32[384,4,2]{0,2,1:T(2,128)S(1)} fusion(f32[4,2,1024,384]{3,2,1,0:T(8,128)} %get-tuple-element.257, f32[384,4,2]{0,2,1:T(2,128)S(1)} %fusion.87, pred[384,1024]{0,1:T(8,128)(4,1)S(1)} %broadcast_compare_fusion.2), kind=kLoop, calls=%fused_computation.8.clone.1 | loop fusion | flops 15725568 | bytes 13000704 | tf_op jit(solution)/shard_map/while/body/eval_jaxpr/reduce_sum | solution.py:55
  175.0 1.5 copy-done
  176.5 3.6 %bitcast_add_fusion.2 = f32[384,4,2,128]{0,3,2,1:T(8,128)S(1)} fusion(f32[384,4,2,128]{0,3,2,1:T(8,128)S(1)} %get-tuple-element.276, bf16[1024,4,128,1]{0,2,3,1:T(8,128)(2,1)S(1)} %bitcast.149, f32[4,2,1024,384]{3,2,1,0:T(8,128)S(1)} %copy-done, f32[384,4,2]{0,2,1:T(2,128)S(1)} %fusion.87, pred[384,1024]{0,1:T(8,128)(4,1)S(1)} %broadcast_compare_fusion.2, ...), kind=kOutput, calls=%fused_computation.11.clone.1 | convolution fusion | flops 822214656 | bytes 17195008 | tf_op jit(solution)/shard_map/while/body/eval_jaxpr/ihcj,jhe->ihce/dot_general | solution.py:56
  180.1 1.7 constant_dynamic-slice_fusion.4
  182.1 6.6 %fusion.86 = (f32[384,4,2]{0,2,1:T(2,128)S(1)}, f32[4,2,1024,384]{3,2,1,0:T(8,128)}) fusion(pred[384,1024]{0,1:T(8,128)(4,1)S(1)} %broadcast_compare_fusion.2, bf16[1024,4,2,64]{0,3,2,1:T(8,128)(2,1)S(1)} %bitcast.148, bf16[384,4,2,64]{0,3,2,1:T(8,128)(2,1)S(1)} %get-tuple-element.290), kind=kOutput, calls=%fused_computation.6.clone.1 | convolution fusion | flops 412087296 | bytes 14430208 | tf_op jit(solution)/shard_map/while/body/eval_jaxpr/ihcd,jhcd->ihcj/dot_general | solution.py:44
  188.8 6.8 %fusion.88 = f32[384,4,2]{0,2,1:T(2,128)S(1)} fusion(f32[4,2,1024,384]{3,2,1,0:T(8,128)} %get-tuple-element.257, f32[384,4,2]{0,2,1:T(2,128)S(1)} %fusion.87, pred[384,1024]{0,1:T(8,128)(4,1)S(1)} %broadcast_compare_fusion.2), kind=kLoop, calls=%fused_computation.8.clone.1 | loop fusion | flops 15725568 | bytes 13000704 | tf_op jit(solution)/shard_map/while/body/eval_jaxpr/reduce_sum | solution.py:55
  195.6 1.5 copy-done
  197.1 3.6 %bitcast_add_fusion.2 = f32[384,4,2,128]{0,3,2,1:T(8,128)S(1)} fusion(f32[384,4,2,128]{0,3,2,1:T(8,128)S(1)} %get-tuple-element.276, bf16[1024,4,128,1]{0,2,3,1:T(8,128)(2,1)S(1)} %bitcast.149, f32[4,2,1024,384]{3,2,1,0:T(8,128)S(1)} %copy-done, f32[384,4,2]{0,2,1:T(2,128)S(1)} %fusion.87, pred[384,1024]{0,1:T(8,128)(4,1)S(1)} %broadcast_compare_fusion.2, ...), kind=kOutput, calls=%fused_computation.11.clone.1 | convolution fusion | flops 822214656 | bytes 17195008 | tf_op jit(solution)/shard_map/while/body/eval_jaxpr/ihcj,jhe->ihce/dot_general | solution.py:56
  201.2 1.0 multiply_convert_fusion
  202.2 6.1 %fusion.38 = bf16[8,1,64,1024]{3,2,1,0:T(8,128)(2,1)} fusion(bf16[1,2048,1024]{2,1,0:T(8,128)(2,1)} %param.27, bf16[8,1,64,2048]{3,2,0,1:T(8,128)(2,1)} %all-gather.11.cloned.1.call-done), kind=kOutput, calls=%fused_computation.43 | convolution fusion | flops 2148007936 | bytes 7340032 | tf_op jit(solution)/shard_map/sxcf,xfd->sxcd/dot_general | solution.py:129
  208.4 3.6 %all-to-all-start.1 = ((bf16[8,1,64,1024]{3,2,1,0:T(8,128)(2,1)}), bf16[8,1,64,1024]{3,2,1,0:T(8,128)(2,1)S(1)}, u32[]{:S(2)}, u32[]{:S(2)}) async-start(bf16[8,1,64,1024]{3,2,1,0:T(8,128)(2,1)} %fusion.38), calls=%async_computation.1 | async-start | bytes 2097152 | tf_op jit(solution)/shard_map/all_to_all | solution.py:136
  212.1 20.6 %all-gather.7.cloned.1.call-done = bf16[1,1,384,2048]{2,3,1,0:T(8,128)(2,1)} async-done(((bf16[1,1,384,512]{2,3,1,0:T(8,128)(2,1)}), bf16[1,1,384,2048]{2,3,1,0:T(8,128)(2,1)}) %all-gather.7.cloned.1.call-update) | async-done | bytes 1572880 | tf_op jit(solution)/shard_map/all_gather | solution.py:122
  232.6 5.4 %fusion.35 = bf16[384,1024]{1,0:T(8,128)(2,1)} fusion(bf16[2048,1024]{1,0:T(8,128)(2,1)} %param.20, bf16[1,1,384,2048]{2,3,1,0:T(8,128)(2,1)} %all-gather.7.cloned.1.call-done), kind=kOutput, calls=%fused_computation.42 | convolution fusion | flops 1611005952 | bytes 6553600 | tf_op jit(solution)/shard_map/dot_general | solution.py:121
  238.4 1.2 gather_fusion.1
  240.2 2.1 multiply_reduce_fusion
  (106 shorter events, 8.1 us)
Async XLA Ops:
  7.2 117.6 %all-gather.9.cloned.1.call-start = ((), (), s32[]{:S(2)}) async-start(), calls=%async_computation.4 | async-start | bytes 5242880 | tf_op jit(solution)/shard_map/all_gather | solution.py:114
  12.6 35.0 %copy-start.8 = (bf16[384,512]{1,0:T(8,128)(2,1)S(1)}, bf16[384,512]{1,0:T(8,128)(2,1)}, u32[]{:S(2)}) copy-start(bf16[384,512]{1,0:T(8,128)(2,1)} %param.17) | copy-start | bytes 1179652
  12.6 72.0 %copy-start.9 = (bf16[384,512]{1,0:T(8,128)(2,1)S(1)}, bf16[384,512]{1,0:T(8,128)(2,1)}, u32[]{:S(2)}) copy-start(bf16[384,512]{1,0:T(8,128)(2,1)} %param.16) | copy-start | bytes 1179652
  12.6 91.4 %copy-start.10 = (f32[4]{0:T(128)S(1)}, f32[4]{0:T(128)}, u32[]{:S(2)}) copy-start(f32[4]{0:T(128)} %param.18) | copy-start | bytes 52
  12.6 91.4 %copy-start.12 = (f32[128]{0:T(128)S(1)}, f32[128]{0:T(128)}, u32[]{:S(2)}) copy-start(f32[128]{0:T(128)} %param.19) | copy-start | bytes 1540
  47.5 91.2 %all-gather.5.cloned.1.call-start = ((), (), s32[]{:S(2)}) async-start(), calls=%async_computation.2 | async-start | bytes 3538944 | tf_op jit(solution)/shard_map/all_gather | solution.py:69
  47.8 9.1 %collective-permute-start = (bf16[384,512]{0,1:T(8,128)(2,1)S(1)}, bf16[384,512]{0,1:T(8,128)(2,1)S(1)}, u32[]{:S(2)}, u32[]{:S(2)}) collective-permute-start(bf16[384,512]{0,1:T(8,128)(2,1)S(1)} %copy.37), channel_id=1, source_target_pairs={{0,4},{4,8},{8,12},{12,16},{16,20},{20,24},{24,28},{28,0},{1,5},{5... | collective-permute-start | bytes 1179656 | tf_op jit(solution)/shard_map/ppermute | solution.py:72
  56.9 9.0 %collective-permute-start.1 = (bf16[384,512]{0,1:T(8,128)(2,1)S(1)}, bf16[384,512]{0,1:T(8,128)(2,1)S(1)}, u32[]{:S(2)}, u32[]{:S(2)}) collective-permute-start(bf16[384,512]{0,1:T(8,128)(2,1)S(1)} %collective-permute-done), channel_id=1, source_target_pairs={{0,4},{4,8},{8,12},{12,16},{16,20},{20,24},{24,28},{28,0},{1,5},{5... | collective-permute-start | bytes 1179656 | tf_op jit(solution)/shard_map/ppermute | solution.py:72
  65.9 9.0 %collective-permute-start.2 = (bf16[384,512]{0,1:T(8,128)(2,1)S(1)}, bf16[384,512]{0,1:T(8,128)(2,1)S(1)}, u32[]{:S(2)}, u32[]{:S(2)}) collective-permute-start(bf16[384,512]{0,1:T(8,128)(2,1)S(1)} %collective-permute-done.1), channel_id=1, source_target_pairs={{0,4},{4,8},{8,12},{12,16},{16,20},{20,24},{24,28},{28,0},{1,5},{5... | collective-permute-start | bytes 1179656 | tf_op jit(solution)/shard_map/ppermute | solution.py:72
  74.9 0.8 copy-start.2
  75.6 9.0 %collective-permute-start.3 = (bf16[384,512]{0,1:T(8,128)(2,1)S(1)}, bf16[384,512]{0,1:T(8,128)(2,1)S(1)}, u32[]{:S(2)}, u32[]{:S(2)}) collective-permute-start(bf16[384,512]{0,1:T(8,128)(2,1)S(1)} %collective-permute-done.2), channel_id=1, source_target_pairs={{0,4},{4,8},{8,12},{12,16},{16,20},{20,24},{24,28},{28,0},{1,5},{5... | collective-permute-start | bytes 1179656 | tf_op jit(solution)/shard_map/ppermute | solution.py:72
  84.6 18.1 %copy-start.4 = (bf16[384,512]{0,1:T(8,128)(2,1)}, bf16[384,512]{0,1:T(8,128)(2,1)S(1)}, u32[]{:S(2)}) copy-start(bf16[384,512]{0,1:T(8,128)(2,1)S(1)} %collective-permute-done.3) | copy-start | bytes 1179652
  84.6 9.0 %collective-permute-start.4 = (bf16[384,512]{0,1:T(8,128)(2,1)S(1)}, bf16[384,512]{0,1:T(8,128)(2,1)S(1)}, u32[]{:S(2)}, u32[]{:S(2)}) collective-permute-start(bf16[384,512]{0,1:T(8,128)(2,1)S(1)} %collective-permute-done.3), channel_id=1, source_target_pairs={{0,4},{4,8},{8,12},{12,16},{16,20},{20,24},{24,28},{28,0},{1,5},{5... | collective-permute-start | bytes 1179656 | tf_op jit(solution)/shard_map/ppermute | solution.py:72
  85.6 116.6 %all-gather.11.cloned.1.call-start = ((), (), s32[]{:S(2)}) async-start(), calls=%async_computation.5 | async-start | bytes 2621440 | tf_op jit(solution)/shard_map/all_gather | solution.py:131
  93.6 9.1 %copy-start.6 = (bf16[384,512]{0,1:T(8,128)(2,1)}, bf16[384,512]{0,1:T(8,128)(2,1)S(1)}, u32[]{:S(2)}) copy-start(bf16[384,512]{0,1:T(8,128)(2,1)S(1)} %collective-permute-done.4) | copy-start | bytes 1179652
  93.6 9.1 %collective-permute-start.5 = (bf16[384,512]{0,1:T(8,128)(2,1)S(1)}, bf16[384,512]{0,1:T(8,128)(2,1)}, u32[]{:S(2)}, u32[]{:S(2)}) collective-permute-start(bf16[384,512]{0,1:T(8,128)(2,1)S(1)} %collective-permute-done.4), channel_id=1, source_target_pairs={{0,4},{4,8},{8,12},{12,16},{16,20},{20,24},{24,28},{28,0},{1,5},{5... | collective-permute-start | bytes 1179656 | tf_op jit(solution)/shard_map/ppermute | solution.py:72
  102.7 9.4 %collective-permute-start.6 = (bf16[384,512]{0,1:T(8,128)(2,1)}, bf16[384,512]{0,1:T(8,128)(2,1)}, u32[]{:S(2)}, u32[]{:S(2)}) collective-permute-start(bf16[384,512]{0,1:T(8,128)(2,1)} %collective-permute-done.5), channel_id=1, source_target_pairs={{0,4},{4,8},{8,12},{12,16},{16,20},{20,24},{24,28},{28,0},{1,5},{5... | collective-permute-start | bytes 1179656 | tf_op jit(solution)/shard_map/ppermute | solution.py:72
  104.0 16.0 %copy-start.7 = (bf16[384,512]{0,1:T(8,128)(2,1)S(1)}, bf16[384,512]{0,1:T(8,128)(2,1)}, u32[]{:S(2)}) copy-start(bf16[384,512]{0,1:T(8,128)(2,1)} %copy-done.6) | copy-start | bytes 1179652
  104.0 16.1 %copy-start.5 = (bf16[384,512]{0,1:T(8,128)(2,1)S(1)}, bf16[384,512]{0,1:T(8,128)(2,1)}, u32[]{:S(2)}) copy-start(bf16[384,512]{0,1:T(8,128)(2,1)} %copy-done.4) | copy-start | bytes 1179652
  104.0 16.2 %copy-start.3 = (bf16[384,512]{0,1:T(8,128)(2,1)S(1)}, bf16[384,512]{0,1:T(8,128)(2,1)}, u32[]{:S(2)}) copy-start(bf16[384,512]{0,1:T(8,128)(2,1)} %copy-done.2) | copy-start | bytes 1179652
  120.4 7.5 %copy-start.14 = (f32[4096]{0:T(1024)S(1)}, f32[4096]{0:T(1024)}, u32[]{:S(2)}) copy-start(f32[4096]{0:T(1024)} %param.22) | copy-start | bytes 49156
  127.9 6.1 %copy-start.1 = (bf16[8,1,64,4096]{3,2,1,0:T(8,128)(2,1)S(1)}, bf16[8,1,64,4096]{3,2,1,0:T(8,128)(2,1)}, u32[]{:S(2)}) copy-start(bf16[8,1,64,4096]{3,2,1,0:T(8,128)(2,1)} %all-gather.9.cloned.1.call-done) | copy-start | bytes 12582916
  127.9 6.1 %copy-start.13 = (bf16[1,4096,512]{2,1,0:T(8,128)(2,1)S(1)}, bf16[1,4096,512]{2,1,0:T(8,128)(2,1)}, u32[]{:S(2)}) copy-start(bf16[1,4096,512]{2,1,0:T(8,128)(2,1)} %param.26) | copy-start | bytes 12582916
  137.3 95.4 %all-gather.7.cloned.1.call-start = ((), (), s32[]{:S(2)}) async-start(), calls=%async_computation.3 | async-start | bytes 1966080 | tf_op jit(solution)/shard_map/all_gather | solution.py:122
  147.5 8.5 %copy-start = (f32[4,2,1024,384]{3,2,1,0:T(8,128)S(1)}, f32[4,2,1024,384]{3,2,1,0:T(8,128)}, u32[]{:S(2)}) copy-start(f32[4,2,1024,384]{3,2,1,0:T(8,128)} %get-tuple-element.257) | copy-start | bytes 37748740 | tf_op jit(solution)/shard_map/while
  168.2 8.3 %copy-start = (f32[4,2,1024,384]{3,2,1,0:T(8,128)S(1)}, f32[4,2,1024,384]{3,2,1,0:T(8,128)}, u32[]{:S(2)}) copy-start(f32[4,2,1024,384]{3,2,1,0:T(8,128)} %get-tuple-element.257) | copy-start | bytes 37748740 | tf_op jit(solution)/shard_map/while
  188.8 8.3 %copy-start = (f32[4,2,1024,384]{3,2,1,0:T(8,128)S(1)}, f32[4,2,1024,384]{3,2,1,0:T(8,128)}, u32[]{:S(2)}) copy-start(f32[4,2,1024,384]{3,2,1,0:T(8,128)} %get-tuple-element.257) | copy-start | bytes 37748740 | tf_op jit(solution)/shard_map/while
  202.2 9.7 %copy-start.11 = (f32[128,2]{0,1:T(2,128)S(1)}, f32[128,2]{0,1:T(2,128)}, u32[]{:S(2)}) copy-start(f32[128,2]{0,1:T(2,128)} %param.24) | copy-start | bytes 3076
  208.4 30.1 %all-to-all-start.1 = ((bf16[8,1,64,1024]{3,2,1,0:T(8,128)(2,1)}), bf16[8,1,64,1024]{3,2,1,0:T(8,128)(2,1)S(1)}, u32[]{:S(2)}, u32[]{:S(2)}) async-start(bf16[8,1,64,1024]{3,2,1,0:T(8,128)(2,1)} %fusion.38), calls=%async_computation.1 | async-start | bytes 2097152 | tf_op jit(solution)/shard_map/all_to_all | solution.py:136
Sparse Core Ops, SparseCore 0:
  47.7 51.4 all-gather.8
  100.8 37.9 all-gather.4
  141.2 34.2 all-gather.10
  202.3 30.2 all-gather.6
